TPU v7x, 512 devices: a whole 4x8x8 slice. The times are simulated.
512 devices in a mesh: kv: 128 (over z, y, core), tp: 4 (over x).
Axes of the slice: x: 4, y: 8, z: 8, core: 2. Of those that a mesh axis runs over, the one named last changes fastest.
Arguments:
- piece_tokens: bfloat16 [512, 2048], P('kv'), may hold values from -6 to 6
- decode_tokens: bfloat16 [128, 2048], P('kv'), may hold values from -6 to 6
- prompt_fill: int32 [1], replicated, may hold values from 16384 to 32256
- decode_fill: int32 [128], P('kv'), may hold values from 1 to 767, 49152 in all
- prompt_cache: bfloat16 [32768, 544], P('kv'), may hold values from -600 to 600
- decode_cache: bfloat16 [128, 768, 544], P('kv'), may hold values from -600 to 600
- input_gain: float32 [2048], replicated, may hold values from 0.1 to 1.9
- query_gain: float32 [768], replicated, may hold values from 0.1 to 1.9
- latent_gain: float32 [512], replicated, may hold values from 0.1 to 1.9
- query_down: bfloat16 [2048, 768], P(None, 'tp'), may hold values from -0.125 to 0.125
- latent_down: bfloat16 [2048, 512], P(None, 'tp'), may hold values from -0.125 to 0.125
- rope_down: bfloat16 [2048, 32], replicated, may hold values from -0.125 to 0.125
- query_up: bfloat16 [768, 1024], P(None, 'tp'), may hold values from -0.21875 to 0.21875
- qrope_up: bfloat16 [768, 512], P(None, 'tp'), may hold values from -0.21875 to 0.21875
- key_up: bfloat16 [16, 64, 512], P('tp'), may hold values from -0.25 to 0.25
- value_up: bfloat16 [16, 512, 64], P('tp'), may hold values from -4 to 4
- out_proj: bfloat16 [1024, 2048], P('tp'), may hold values from -4 to 4
Outputs:
- piece_out: bfloat16 [512, 2048], P('kv')
- decode_out: bfloat16 [128, 2048], P('kv')
- piece_rows: bfloat16 [512, 544], P('kv')
- decode_rows: bfloat16 [128, 544], P('kv')
Inputs may be any that keep to these rules, and one draw needn't show every extreme that they name: `prompt_fill`: the piece takes the 512 positions that follow the cache's filled positions. `decode_fill`: a decoding sequence's new token takes the position that follows its filled ones.
All inputs are finite; a program needn't handle non-finite values. No bound on the sum of `decode_fill` on one device may be relied on, other than what follows from the above.
Results may differ from a plain program's by a relative error of at most 0.035.
Values may be sent and summed in bfloat16 or wider, within the bound.
A program may use at most 64 MiB of HBM per device.

v0:
```python
import jax
import jax.numpy as jnp
from jax import lax
from jax.sharding import PartitionSpec as P

NOPE = 64
ROPE = 32


NEG_FILL = -1e30
RMS_EPS = 1e-06
THETA = 10000.0


def laid_out(parts, dim):
    shape = list(parts.shape[1:])
    shape[dim] *= parts.shape[0]
    return jnp.moveaxis(parts, 0, dim).reshape(shape)


def gather_packed(arrays, axis, dims):
    flat = jnp.concatenate([a.reshape(-1) for a in arrays])
    lines, at, finished = (lax.all_gather(flat, axis), 0, [])
    for a, dim in zip(arrays, dims):
        parts = lines[:, at : at + a.size].reshape(-1, *a.shape)
        finished.append(laid_out(parts, dim))
        at += a.size
    return tuple(finished)


def sent_together(arrays, axis, split_dim, concat_dim, along):
    widths = [a.shape[along] for a in arrays]
    both = jnp.concatenate(arrays, axis=along)
    filled = lax.all_to_all(both, axis, split_axis=split_dim, concat_axis=concat_dim, tiled=True)
    return tuple(jnp.split(filled, [sum(widths[:k]) for k in range(1, len(widths))], axis=along))


def from_everyone(shard, axis):
    copies = jnp.broadcast_to(shard, (lax.axis_size(axis), *shard.shape))
    return lax.all_to_all(copies, axis, split_axis=0, concat_axis=0, tiled=True)


def over_copies(shard, axis):
    everything = from_everyone(shard, axis)
    return jnp.sum(everything.astype(jnp.float32), axis=0)


def rms_scale(values, gain_row):
    widened = values.astype(jnp.float32)
    scaled = (
        widened
        * lax.rsqrt(jnp.mean(widened * widened, axis=-1, keepdims=True) + RMS_EPS)
        * gain_row
    )
    return scaled.astype(jnp.bfloat16)


def rotate(values, places):
    half_width = values.shape[-1] // 2
    inverse = THETA ** (-jnp.arange(half_width, dtype=jnp.float32) / half_width)
    angles = places.astype(jnp.float32)[..., None] * inverse
    first_half = values[..., :half_width].astype(jnp.float32)
    second_half = values[..., half_width:].astype(jnp.float32)
    cosine = jnp.cos(angles)
    sine_part = jnp.sin(angles)
    return jnp.concatenate(
        [
            first_half * cosine - second_half * sine_part,
            first_half * sine_part + second_half * cosine,
        ],
        axis=-1,
    ).astype(jnp.bfloat16)


def make_queries(query_lat, places, query_up, qrope_up, key_up):
    row_count = query_lat.shape[0]
    head_count = key_up.shape[0]
    nope_part = (
        jnp.dot(query_lat, query_up, preferred_element_type=jnp.float32)
        .astype(jnp.bfloat16)
        .reshape(row_count, head_count, -1)
    )
    rope_raw = (
        jnp.dot(query_lat, qrope_up, preferred_element_type=jnp.float32)
        .astype(jnp.bfloat16)
        .reshape(row_count, head_count, -1)
    )
    turned = rotate(rope_raw, places[:, None])
    absorbed = jnp.einsum(
        "nhc,hcl->nhl", nope_part, key_up, preferred_element_type=jnp.float32
    ).astype(jnp.bfloat16)
    return (absorbed, turned)


def block_attend(absorbed, turned, key_rows, key_places, query_places, value_up):
    latent_width = value_up.shape[1]
    score_scale = (NOPE + ROPE) ** (-0.5)
    latent_keys = key_rows[:, :latent_width]
    scores = (
        jnp.einsum("nhl,sl->nhs", absorbed, latent_keys, preferred_element_type=jnp.float32)
        + jnp.einsum(
            "nhr,sr->nhs", turned, key_rows[:, latent_width:], preferred_element_type=jnp.float32
        )
    ) * score_scale
    allowed = key_places[None, None, :] <= query_places[:, None, None]
    scores = jnp.where(allowed, scores, NEG_FILL)
    local_peak = jnp.max(scores, axis=-1)
    exp_scores = jnp.where(allowed, jnp.exp(scores - local_peak[..., None]), 0.0)
    weight_sum = jnp.sum(exp_scores, axis=-1)
    weights = exp_scores.astype(jnp.bfloat16)
    mixed_rows = jnp.einsum("nhs,sl->nhl", weights, latent_keys, preferred_element_type=jnp.float32)
    partial_sum = jnp.einsum(
        "nhl,hlv->nhv", mixed_rows, value_up.astype(jnp.float32), precision=lax.Precision.HIGHEST
    )
    return (partial_sum, weight_sum, local_peak)


def insert_row(cache_rows, new_row, fill_one):
    return lax.dynamic_update_slice(cache_rows, new_row[None], (fill_one, jnp.zeros((), jnp.int32)))


def local(
    piece_tokens,
    decode_tokens,
    prompt_fill,
    decode_fill,
    prompt_cache,
    decode_cache,
    input_gain,
    query_gain,
    latent_gain,
    query_down,
    latent_down,
    rope_down,
    query_up,
    qrope_up,
    key_up,
    value_up,
    out_proj,
):
    kv_index = lax.axis_index("kv")
    piece_dev = piece_tokens.shape[0]
    shard_len = prompt_cache.shape[0]
    fill_start = prompt_fill[0]
    own_places = fill_start + kv_index * piece_dev + jnp.arange(piece_dev, dtype=jnp.int32)
    places = jnp.concatenate([own_places, decode_fill])
    tokens = jnp.concatenate([piece_tokens, decode_tokens], axis=0)
    normed = rms_scale(tokens, input_gain)
    query_comp = jnp.dot(normed, query_down, preferred_element_type=jnp.float32).astype(
        jnp.bfloat16
    )
    latent_comp = jnp.dot(normed, latent_down, preferred_element_type=jnp.float32).astype(
        jnp.bfloat16
    )
    query_comp, latent_comp = gather_packed((query_comp, latent_comp), "tp", (1, 1))
    query_lat = rms_scale(query_comp, query_gain)
    rope_raw = jnp.dot(normed, rope_down, preferred_element_type=jnp.float32).astype(jnp.bfloat16)
    new_rows = jnp.concatenate(
        [rms_scale(latent_comp, latent_gain), rotate(rope_raw, places)], axis=-1
    )
    piece_rows = new_rows[:piece_dev]
    decode_rows = new_rows[piece_dev:]
    decode_absorbed, decode_turned = make_queries(
        query_lat[piece_dev:], decode_fill, query_up, qrope_up, key_up
    )
    piece_latent, arrived = gather_packed((query_lat[:piece_dev], piece_rows), "kv", (0, 0))
    arrived_places = fill_start + jnp.arange(arrived.shape[0], dtype=jnp.int32)
    piece_absorbed, piece_turned = make_queries(
        piece_latent, arrived_places, query_up, qrope_up, key_up
    )
    piece_total = arrived.shape[0]
    query_places = fill_start + jnp.arange(piece_total, dtype=jnp.int32)
    zero_rows = jnp.zeros((shard_len, arrived.shape[1]), arrived.dtype)
    padded = jnp.concatenate([zero_rows, arrived, zero_rows], axis=0)
    offset = jnp.clip(kv_index * shard_len - fill_start + shard_len, 0, piece_total + shard_len)
    window = lax.dynamic_slice_in_dim(padded, offset, shard_len, 0)
    key_places = kv_index * shard_len + jnp.arange(shard_len, dtype=jnp.int32)
    fresh_rows = (key_places >= fill_start) & (key_places < fill_start + piece_total)
    key_rows = jnp.where(fresh_rows[:, None], window, prompt_cache)
    partial_sum, weight_sum, local_peak = block_attend(
        piece_absorbed, piece_turned, key_rows, key_places, query_places, value_up
    )
    all_parts, all_totals, all_peaks = sent_together(
        (partial_sum.reshape(1, piece_total, -1), weight_sum[None], local_peak[None]), "kv", 1, 0, 2
    )
    global_peak = jnp.max(all_peaks, axis=0)
    factor = jnp.exp(all_peaks - global_peak[None])
    merged = jnp.sum(all_parts.reshape(all_peaks.shape + (-1,)) * factor[..., None], axis=0)
    denominator = jnp.sum(all_totals * factor, axis=0)
    piece_value = (merged / denominator[..., None]).astype(jnp.bfloat16)
    decode_keys = jax.vmap(insert_row)(decode_cache, decode_rows, decode_fill)

    def attend_one(absorbed_one, turned_one, keys_one, fill_one):
        cache_places = jnp.arange(keys_one.shape[0], dtype=jnp.int32)
        return block_attend(
            absorbed_one[None], turned_one[None], keys_one, cache_places, fill_one[None], value_up
        )

    decode_part, decode_total, decode_peak = jax.vmap(attend_one)(
        decode_absorbed, decode_turned, decode_keys, decode_fill
    )
    decode_value = (decode_part[:, 0] / decode_total[:, 0, :, None]).astype(jnp.bfloat16)
    values = jnp.concatenate([piece_value, decode_value], axis=0)
    values = values.reshape(values.shape[0], -1)
    partial_value = jnp.dot(values, out_proj, preferred_element_type=jnp.float32).astype(
        jnp.bfloat16
    )
    summed = over_copies(partial_value, "tp").astype(jnp.float32).astype(jnp.bfloat16)
    return (summed[:piece_dev], summed[piece_dev:], piece_rows, decode_rows)


def solution(mesh):
    placed = (
        P("kv", None),
        P("kv", None),
        P(),
        P("kv"),
        P("kv", None),
        P("kv", None, None),
        P(),
        P(),
        P(),
        P(None, "tp"),
        P(None, "tp"),
        P(),
        P(None, "tp"),
        P(None, "tp"),
        P("tp", None, None),
        P("tp", None, None),
        P("tp", None),
    )
    return jax.shard_map(
        local,
        mesh=mesh,
        in_specs=placed,
        out_specs=(P("kv", None), P("kv", None), P("kv", None), P("kv", None)),
        check_vma=False,
    )
```

profile of v0, /device:TPU:1, one launch (start us, length us, event | category | flops | bytes accessed | tf_op | source)
XLA Modules:
  0.0 198.0 jit_solution(13090020181358731536)
XLA Ops:
  7.3 1.3 copy.110
  8.6 0.9 fusion.32
  9.6 1.5 convolution_convert_fusion.3
  11.2 0.2 fusion.11
  11.5 1.3 dynamic-slice.11
  13.5 0.3 dynamic-update-slice.3
  13.8 13.9 %all-reduce = bf16[6400]{0:T(1024)(128)(2,1)S(1)} all-reduce(bf16[6400]{0:T(1024)(128)(2,1)S(1)} %dynamic-update-slice.3), channel_id=2, replica_groups=mesh['kv'=128,'tp'=4] {'tp'}, use_global_device_ids=true, to_apply=%add | all-reduce | flops 6400 | bytes 25600
  29.5 1.1 convolution_convert_fusion.5
  31.6 0.6 reshape.434
  32.2 0.9 copy.75
  33.2 0.6 fusion.75
  33.8 0.8 constant_dynamic-slice_fusion
  34.7 2.0 %and_reduce_fusion = pred[]{:T(512)} fusion(s32[3]{0:T(128)S(1)} %copy-done.16, s32[1]{0:T(128)} %bitcast.22, s32[1]{0:T(128)} %bitcast.21, s32[1]{0:T(128)} %constant.80.clone.1), kind=kLoop, calls=%fused_computation.114 | loop fusion | flops 17 | bytes 25 | tf_op jit(solution)/shard_map/reduce.1
  36.7 1.2 broadcast_select_fusion
  38.1 1.6 scatter.4
  40.5 0.8 broadcast_compare_fusion
  41.3 1.1 fusion.79
  42.4 0.2 fusion.18
  42.6 79.9 %all-gather.5.cloned.1.call-done = bf16[128,1,5248]{2,1,0:T(2,128)(2,1)} async-done(((bf16[1,1,5248]{2,1,0:T(2,128)(2,1)}), bf16[128,1,5248]{2,1,0:T(2,128)(2,1)}) %all-gather.5.cloned.1.call-update) | async-done | bytes 1343504 | tf_op jit(solution)/shard_map/all_gather | solution.py:23
  122.5 1.9 copy.104
  124.6 0.5 reshape_reshape.6
  125.1 0.4 convolution_convert_fusion.2
  125.5 2.1 %convolution_convert_fusion.1 = bf16[512,256]{0,1:T(8,128)(2,1)} fusion(bf16[512,768]{1,0:T(8,128)(2,1)S(1)} %reshape_reshape.6, bf16[768,256]{1,0:T(8,128)(2,1)} %param.31), kind=kOutput, calls=%fused_computation.13 | convolution fusion | flops 201457664 | bytes 1441792 | tf_op jit(solution)/shard_map/dot_general | solution.py:79
  127.6 0.7 reshape_reshape.7
  128.4 0.9 fusion.22
  129.3 1.8 fusion.28
  131.0 3.2 %fusion.77 = (f32[512,4]{0,1:T(4,128)S(1)}, f32[512,4,256]{0,2,1:T(8,128)S(1)}) fusion(f32[512,4,256]{0,2,1:T(8,128)} %fusion.28, bf16[256,544]{1,0:T(8,128)(2,1)S(1)} %fusion.22, bf16[512,4,64]{0,2,1:T(8,128)(2,1)} %bitcast.107, bf16[4,64,512]{2,1,0:T(8,128)(2,1)} %param.33, pred[512,256]{0,1:T(8,128)(4,1)} %broadcast_compare_fusion), kind=kOutput, calls=%fused_computation.141 | convolution fusion | flops 674232320 | bytes 5120000 | tf_op jit(solution)/shard_map/nhl,sl->nhs/dot_general | solution.py:100
  134.3 1.7 fusion.13
  136.0 0.4 fusion.5
  136.4 0.5 copy-done.9
  137.0 2.2 %fusion.78 = f32[4,512,64]{1,2,0:T(8,128)S(1)} fusion(f32[512,4,512]{2,0,1:T(8,128)S(1)} %fusion.13, bf16[4,512,64]{1,2,0:T(8,128)(2,1)S(1)} %copy-done.9), kind=kOutput, calls=%fused_computation.142 | convolution fusion | flops 805306368 | bytes 4980736 | tf_op jit(solution)/shard_map/nhl,hlv->nhv/dot_general | solution.py:112
  139.2 0.4 copy.78
  140.0 1.9 pad_maximum_fusion
  141.9 9.7 %all-to-all-start = ((f32[1,512,264]{2,0,1:T(1,128)}), f32[1,512,264]{2,0,1:T(1,128)S(1)}, u32[]{:S(2)}, u32[]{:S(2)}) async-start(f32[1,512,264]{2,0,1:T(1,128)} %pad_maximum_fusion), calls=%async_computation | async-start | bytes 1572864 | tf_op jit(solution)/shard_map/all_to_all | solution.py:34
  151.6 0.3 fusion.76
  152.1 0.3 convolution_bitcast_fusion
  152.4 0.3 fusion.37
  152.9 24.6 %all-to-all-done = f32[1,512,264]{2,0,1:T(1,128)S(1)} async-done(((f32[1,512,264]{2,0,1:T(1,128)}), f32[1,512,264]{2,0,1:T(1,128)S(1)}, u32[]{:S(2)}, u32[]{:S(2)}) %all-to-all-start) | async-done | bytes 540704 | tf_op jit(solution)/shard_map/all_to_all | solution.py:34
  177.5 1.9 reduce.21
  179.4 0.2 all_to_all.13
  179.6 0.2 slice_reduce_fusion
  179.8 0.2 fusion.23
  180.2 0.2 copy.82
  180.4 0.2 fusion.19
  180.8 0.2 convolution_convert_fusion
  181.1 8.8 %all_to_all.17 = bf16[4,5,2048]{2,1,0:T(8,128)(2,1)S(1)} all-to-all(bf16[4,5,2048]{2,1,0:T(8,128)(2,1)S(1)} %broadcast_in_dim.94), channel_id=1, replica_groups=mesh['kv'=128,'tp'=4] {'tp'}, dimensions={0} | all-to-all | bytes 163840 | tf_op jit(solution)/shard_map/all_to_all | solution.py:40
  190.0 0.6 slice.124
  190.6 0.6 slice.125
  (98 shorter events, 4.1 us)
Async XLA Ops:
  7.2 173.7 %copy-start = (bf16[256,2048]{1,0:T(8,128)(2,1)S(1)}, bf16[256,2048]{1,0:T(8,128)(2,1)}, u32[]{:S(2)}) copy-start(bf16[256,2048]{1,0:T(8,128)(2,1)} %param.35) | copy-start | bytes 3145732
  7.2 26.0 %copy-start.17 = (s32[1,2]{1,0:T(1,128)S(1)}, s32[1,2]{1,0:T(1,128)}, u32[]{:S(2)}) copy-start(s32[1,2]{1,0:T(1,128)} %constant.83.clone.1) | copy-start | bytes 28
  7.2 27.5 %copy-start.16 = (s32[3]{0:T(128)S(1)}, s32[3]{0:T(128)}, u32[]{:S(2)}) copy-start(s32[3]{0:T(128)} %constant.84.clone.1) | copy-start | bytes 40
  7.2 4.0 %copy-start.10 = (bf16[4,2048]{1,0:T(4,128)(2,1)S(1)}, bf16[4,2048]{1,0:T(4,128)(2,1)}, u32[]{:S(2)}) copy-start(bf16[4,2048]{1,0:T(4,128)(2,1)} %param.19) | copy-start | bytes 49156
  7.2 4.0 %copy-start.11 = (bf16[1,2048]{1,0:T(2,128)(2,1)S(1)}, bf16[1,2048]{1,0:T(2,128)(2,1)}, u32[]{:S(2)}) copy-start(bf16[1,2048]{1,0:T(2,128)(2,1)} %param.20) | copy-start | bytes 12292
  7.2 25.0 %copy-start.8 = (bf16[256,544]{0,1:T(8,128)(2,1)S(1)}, bf16[256,544]{0,1:T(8,128)(2,1)}, u32[]{:S(2)}) copy-start(bf16[256,544]{0,1:T(8,128)(2,1)} %param.23) | copy-start | bytes 835588
  7.2 4.0 %copy-start.12 = (f32[2048]{0:T(1024)S(1)}, f32[2048]{0:T(1024)}, u32[]{:S(2)}) copy-start(f32[2048]{0:T(1024)} %param.25) | copy-start | bytes 24580
  7.3 24.2 %copy-start.14 = (f32[768]{0:T(1024)S(1)}, f32[768]{0:T(1024)}, u32[]{:S(2)}) copy-start(f32[768]{0:T(1024)} %param.26) | copy-start | bytes 9220
  7.3 23.4 %copy-start.15 = (f32[512]{0:T(512)S(1)}, f32[512]{0:T(512)}, u32[]{:S(2)}) copy-start(f32[512]{0:T(512)} %param.27) | copy-start | bytes 6148
  7.3 3.9 %copy-start.7 = (bf16[2048,128]{1,0:T(8,128)(2,1)S(1)}, bf16[2048,128]{1,0:T(8,128)(2,1)}, u32[]{:S(2)}) copy-start(bf16[2048,128]{1,0:T(8,128)(2,1)} %param.29) | copy-start | bytes 1572868
  7.3 115.2 %all-gather.5.cloned.1.call-start = ((), (), s32[]{:S(2)}) async-start(), calls=%async_computation.2 | async-start | bytes 2707968 | tf_op jit(solution)/shard_map/all_gather | solution.py:23
  8.6 31.1 %copy-start.3 = (bf16[768,256]{1,0:T(8,128)(2,1)S(1)}, bf16[768,256]{1,0:T(8,128)(2,1)}, u32[]{:S(2)}) copy-start(bf16[768,256]{1,0:T(8,128)(2,1)} %param.31) | copy-start | bytes 1179652
  8.6 31.3 %copy-start.6 = (bf16[768,128]{1,0:T(8,128)(2,1)S(1)}, bf16[768,128]{1,0:T(8,128)(2,1)}, u32[]{:S(2)}) copy-start(bf16[768,128]{1,0:T(8,128)(2,1)} %param.32) | copy-start | bytes 589828
  31.0 93.4 %copy-start.13 = (bf16[4,544]{1,0:T(4,128)(2,1)}, bf16[4,544]{1,0:T(4,128)(2,1)S(1)}, u32[]{:S(2)}) copy-start(bf16[4,544]{1,0:T(4,128)(2,1)S(1)} %slice.114) | copy-start | bytes 13060
  39.7 84.7 %copy-start.1 = (bf16[1,768,544]{1,2,0:T(8,128)(2,1)}, bf16[1,768,544]{1,2,0:T(8,128)(2,1)S(1)}, u32[]{:S(2)}) copy-start(bf16[1,768,544]{1,2,0:T(8,128)(2,1)S(1)} %scatter.4) | copy-start | bytes 2506756
  125.0 3.4 %copy-start.4 = (bf16[256,544]{1,0:T(8,128)(2,1)S(1)}, bf16[256,544]{1,0:T(8,128)(2,1)}, u32[]{:S(2)}) copy-start(bf16[256,544]{1,0:T(8,128)(2,1)} %copy.75) | copy-start | bytes 835588
  134.3 1.7 copy-start.5
  136.0 1.0 copy-start.9
  139.6 12.0 %copy-start.2 = (bf16[1,768,544]{1,2,0:T(8,128)(2,1)S(1)}, bf16[1,768,544]{1,2,0:T(8,128)(2,1)}, u32[]{:S(2)}) copy-start(bf16[1,768,544]{1,2,0:T(8,128)(2,1)} %copy-done.1) | copy-start | bytes 2506756
  141.9 35.6 %all-to-all-start = ((f32[1,512,264]{2,0,1:T(1,128)}), f32[1,512,264]{2,0,1:T(1,128)S(1)}, u32[]{:S(2)}, u32[]{:S(2)}) async-start(f32[1,512,264]{2,0,1:T(1,128)} %pad_maximum_fusion), calls=%async_computation | async-start | bytes 1572864 | tf_op jit(solution)/shard_map/all_to_all | solution.py:34
Sparse Core Ops, SparseCore 0:
  32.3 90.1 all-gather.4
where the time goes:
time: 199 us; the launch traced here: 198 us
  waiting for transfers between devices  104 us (52%)
  blocking collectives  22.7 us (11%)
  matrix products  17.1 us (9%)
  between operations  16.5 us (8%)
  local copies, waits for them, and re-layouts  15.1 us (8%)
  other arithmetic  12.4 us (6%)
  starting transfers between devices  9.7 us (5%)
    all_gather x1, waiting for transfers between devices, gather_packed(): lines, at, finished = (lax.all_gather(flat, axis), 0, [])  79.9 us
    all_to_all x1, waiting for transfers between devices, sent_together(): lax.all_to_all(both, axis, split_axis=split_dim, concat_axis=concat_dim,...  24.6 us
    unnamed x1, blocking collectives  13.9 us
    all_to_all x1, starting transfers between devices, sent_together(): lax.all_to_all(both, axis, split_axis=split_dim, concat_axis=concat_dim,...  9.66 us
    all_to_all x1, blocking collectives, from_everyone(): return lax.all_to_all(copies, axis, split_axis=0, concat_axis=0, tiled=True)  8.8 us
    unnamed x44, local copies, waits for them, and re-layouts  7.06 us
  transfers between devices with their start and end apart: 2, of which 2 were waited for; matrix products, arithmetic and copies ran while one was open for 6% of the time, Pallas kernels for 0%

commit v1 on v0

v1 whole, which is shorter than its diff:
```python
import functools

import jax
import jax.numpy as jnp
from jax import lax
from jax.experimental import pallas as pl
from jax.experimental.pallas import tpu as pltpu
from jax.sharding import PartitionSpec as P

MESH = pl.DeviceIdType.MESH
NEG = -1e30
EPS = 1e-06
LOG2E = 1.4426950408889634
SCALE = (64 + 32) ** (-0.5) * LOG2E
INVERSE = tuple(float(10000.0 ** (-i / 16)) for i in range(16))
BF = jnp.bfloat16
F32 = jnp.float32


def dot(a, b):
    return jnp.dot(a, b, preferred_element_type=F32)


def dot_t(a, b):
    return lax.dot_general(a, b, (((1,), (1,)), ((), ())), preferred_element_type=F32)


def angles(places):
    lane = lax.broadcasted_iota(jnp.int32, (8, 128), 1)
    step = lax.rem(lane, 16)
    inverse = jnp.full((8, 128), INVERSE[0], F32)
    for i in range(1, 16):
        inverse = jnp.where(step == i, INVERSE[i], inverse)
    turn = places.astype(F32) * inverse
    sine = jnp.sin(turn)
    return jnp.cos(turn), jnp.where(lax.rem(lane, 32) < 16, -sine, sine)


def rotate(values, cosine, sine):
    lane = lax.broadcasted_iota(jnp.int32, (8, 128), 1)
    other = jnp.where(
        lax.rem(lane, 32) < 16, pltpu.roll(values, 112, 1), pltpu.roll(values, 16, 1)
    )
    return values * cosine + other * sine


def kernel(
    nz, ny, ntp,
    fill_any, dfill_any, piece_any, dec_any, ingain_any, qgain_any, lgain_any,
    qd_any, ld_any, rd_any, qu_any, qr_any, ku_any, vu_any, op_any, pc_any, dc_any,
    piece_out, dec_out, piece_rows, dec_rows,
    fill_v, dfill_v, piece_v, dec_v, ingain_v, qgain_v, lgain_v,
    qd, ld, rd, qu, qr, ku, vu, op, pc, dc,
    partner, xs, cbuf, nb, qs, kbuf, vbuf, qbuf, rsend, rbuf, mid, vs, obuf, dbuf,
    chip_in, line_in, all_in,
    load_sem, c_send, c_recv, p_send, p_recv, n_send, n_recv,
    q_send, q_recv, r_send, r_recv, o_send, o_recv, d_send, d_recv,
):
    kv, tp = lax.axis_index("kv"), lax.axis_index("tp")
    chip, core = lax.div(kv, 2), lax.rem(kv, 2)
    z, y = lax.div(chip, ny), lax.rem(chip, ny)
    peers = nz * ny - 1
    other_kv = chip * 2 + (1 - core)

    pairs = (
        (piece_any, piece_v), (dec_any, dec_v), (ingain_any, ingain_v), (qd_any, qd),
        (ld_any, ld), (pc_any, pc), (ku_any, ku), (vu_any, vu), (rd_any, rd),
        (fill_any, fill_v), (dfill_any, dfill_v), (qgain_any, qgain_v), (lgain_any, lgain_v),
        (qu_any, qu), (qr_any, qr), (dc_any, dc), (op_any, op),
    )
    loads = [pltpu.make_async_copy(a, v, load_sem.at[i]) for i, (a, v) in enumerate(pairs)]
    for load in loads:
        load.start()

    barrier = pltpu.get_barrier_semaphore()

    z_part = [lax.rem(z + d, nz) * (2 * ny) + core for d in range(nz)]
    y_part = [lax.rem(y + d, ny) * 2 for d in range(ny)]

    def targets():
        def far(step):
            dz, dy = step
            return -(min(dz, nz - dz) + min(dy, ny - dy))

        steps = [(dz, dy) for dz in range(nz) for dy in range(ny)][1:]
        for dz, dy in sorted(steps, key=far):
            yield z_part[dz] + y_part[dy], dz * ny + dy, (-dz % nz) * ny + -dy % ny

    def tell(sem, kv_t, tp_t):
        pl.semaphore_signal(sem, inc=1, device_id=(kv_t, tp_t), device_id_type=MESH)

    @pl.when(core == 0)
    def _():
        for j in range(1, ntp):
            tell(barrier, kv, lax.rem(tp + j, ntp))
        pl.semaphore_wait(barrier, ntp)
        tell(chip_in, other_kv, tp)
        for j in range(1, ntp):
            tell(line_in, kv, lax.rem(tp + j, ntp))

    @pl.when(core == 1)
    def _():
        tell(barrier, other_kv, tp)
        pl.semaphore_wait(chip_in, 1)
        for kv_t, unused, unused_too in targets():
            tell(barrier, kv_t, tp)

    xs[...] = jnp.zeros(xs.shape, F32)
    for load in loads[:5]:
        load.wait()
    xs[0:4] = piece_v[...].astype(F32)
    xs[4:5] = dec_v[...].astype(F32)
    x = xs[...]
    mean = jnp.mean(x * x, axis=-1, keepdims=True)
    normed = (x * lax.rsqrt(mean + EPS) * ingain_v[...]).astype(BF)
    cbuf[tp, :, 0:128] = dot(normed, ld[...]).astype(BF)
    cbuf[tp, :, 128:320] = dot_t(normed, qd[...]).astype(BF)

    zeros = jnp.zeros((32, kbuf.shape[2]), BF)
    row = lax.broadcasted_iota(jnp.int32, (64, vbuf.shape[2]), 0)
    ones = jnp.where((row == 0) | (row == 4), 1.0, 0.0).astype(BF)
    for h in range(4):
        kbuf[h, 96:128] = zeros
        vbuf[h, 64:128] = ones
    nb[0:16] = jnp.zeros((16, 640), BF)
    nb[32:128] = jnp.zeros((96, 640), BF)
    for load in loads[5:9]:
        load.wait()

    def expand(rows, at):
        latent = rows[0:512]
        keys = dot(ku[...], latent).astype(BF)
        vals = dot(vu[...], latent).astype(BF)
        turned_keys = rows[512:544]
        for h in range(4):
            kbuf[h, 0:64, at : at + 256] = keys[64 * h : 64 * h + 64]
            kbuf[h, 64:96, at : at + 256] = turned_keys
            vbuf[h, 0:64, at : at + 256] = vals[64 * h : 64 * h + 64]

    expand(pc, 0)
    rope_raw = dot_t(normed, rd[...]).astype(BF).astype(F32)
    for load in loads[9:]:
        load.wait()
    fill, dfill = fill_v[...], dfill_v[...]
    token_row = lax.broadcasted_iota(jnp.int32, (8, 128), 0)
    places = jnp.where(token_row < 4, fill + kv * 4 + token_row, dfill)
    cosine, sine = angles(places)
    rope_row = rotate(
        jnp.concatenate([rope_raw, jnp.zeros((8, 96), F32)], axis=1), cosine, sine
    ).astype(BF)

    @pl.when(core == 0)
    def _():
        pl.semaphore_wait(line_in, ntp - 1)
        tell(chip_in, other_kv, tp)

    @pl.when(core == 1)
    def _():
        pl.semaphore_wait(chip_in, 1)

    def to_tp(src, dst, send, recv):
        copies = []
        for j in range(1, ntp):
            copies.append(
                pltpu.make_async_remote_copy(
                    src_ref=src, dst_ref=dst, send_sem=send, recv_sem=recv,
                    device_id=(kv, lax.rem(tp + j, ntp)), device_id_type=MESH,
                )
            )
            copies[-1].start()

    def to_partner(src, dst, send, recv):
        return pltpu.make_async_remote_copy(
            src_ref=src, dst_ref=dst, send_sem=send, recv_sem=recv,
            device_id=(other_kv, tp), device_id_type=MESH,
        )

    def many(ref, send, recv):
        return to_partner(ref, ref, send, recv)

    to_tp(cbuf.at[tp], cbuf.at[tp], c_send, c_recv)
    swap_cache = to_partner(pc, partner, p_send, p_recv)
    swap_cache.start()
    many(cbuf.at[pl.ds(0, ntp - 1)], c_send, c_recv).wait_recv()

    parts = [cbuf[j] for j in range(ntp)]
    lat = [p[:, 0:128].astype(F32) for p in parts]
    com = [p[:, 128:320].astype(F32) for p in parts]
    lat_mean = sum(jnp.sum(v * v, axis=-1, keepdims=True) for v in lat) / (128.0 * ntp)
    com_mean = sum(jnp.sum(v * v, axis=-1, keepdims=True) for v in com) / (192.0 * ntp)
    lat_scale, com_scale = lax.rsqrt(lat_mean + EPS), lax.rsqrt(com_mean + EPS)
    nope = jnp.zeros((8, 256), F32)
    turned = jnp.zeros((8, 128), F32)
    for j in range(ntp):
        part = (com[j] * com_scale * qgain_v[192 * j : 192 * j + 192][None]).astype(BF)
        nope += dot(part, qu[192 * j : 192 * j + 192])
        turned += dot(part, qr[192 * j : 192 * j + 192])
    turned = rotate(turned.astype(BF).astype(F32), cosine, sine) * SCALE
    nope = nope * SCALE
    for h in range(4):
        qs[pl.ds(h, 8, stride=4), :] = jnp.concatenate(
            [
                nope[:, 64 * h : 64 * h + 64],
                turned[:, 32 * h : 32 * h + 32],
                jnp.zeros((8, 32), F32),
            ],
            axis=1,
        )
    qbuf[0] = qs[0:16].astype(BF)

    @pl.when(core == 0)
    def _():
        pl.semaphore_wait(all_in, 1)

    @pl.when(core == 1)
    def _():
        pl.semaphore_wait(barrier, peers)
        tell(all_in, other_kv, tp)

    for kv_t, unused, slot in targets():
        pltpu.make_async_remote_copy(
            src_ref=qbuf.at[0], dst_ref=qbuf.at[slot], send_sem=q_send, recv_sem=q_recv,
            device_id=(kv_t, tp), device_id_type=MESH,
        ).start()

    for j in range(ntp):
        rows = (lat[j] * lat_scale * lgain_v[:, 128 * j : 128 * j + 128]).astype(BF)
        nb[0:8, 128 * j : 128 * j + 128] = rows
        piece_rows[:, 128 * j : 128 * j + 128] = rows[0:4]
        dec_rows[:, 128 * j : 128 * j + 128] = rows[4:5]
    nb[0:8, 512:640] = rope_row
    piece_rows[:, 512:544] = rope_row[0:4, 0:32]
    dec_rows[:, 512:544] = rope_row[4:5, 0:32]
    swap_rows = to_partner(nb.at[pl.ds(0, 16)], nb.at[pl.ds(16, 16)], n_send, n_recv)
    swap_rows.start()

    head = lax.broadcasted_iota(jnp.int32, (8, 256), 0)
    mine = lax.div(lax.broadcasted_iota(jnp.int32, (8, 256), 1), 64) == head
    alone = jnp.where(mine, jnp.broadcast_to(nope[4:5], (8, 256)), 0.0).astype(BF)
    absorbed = dot(alone, ku[...]).astype(BF)
    dec_turned = qs[16:24, 64:96].astype(BF)
    scores = dot(absorbed, dc[0:512]) + dot(dec_turned, dc[512:544])
    spot = lax.broadcasted_iota(jnp.int32, scores.shape, 1)
    scores = jnp.where(spot < dfill, scores, NEG)
    new_lat = nb[0:8, 0:512].astype(F32)[4:5]
    new_rope = rope_row.astype(F32)[4:5, 0:32]
    new_score = jnp.sum(absorbed.astype(F32) * new_lat, axis=-1, keepdims=True) + jnp.sum(
        dec_turned.astype(F32) * new_rope, axis=-1, keepdims=True
    )
    peak = jnp.maximum(jnp.max(scores, axis=-1, keepdims=True), new_score)
    weights = jnp.exp2(scores - peak)
    new_weight = jnp.exp2(new_score - peak)
    total = jnp.sum(weights, axis=-1, keepdims=True) + new_weight
    mixed = dot_t(weights.astype(BF), dc[0:512]) + new_weight * new_lat
    value = dot_t(mixed.astype(BF), vu[...]) / total
    value = jnp.sum(jnp.where(mine, value, 0.0), axis=0, keepdims=True)
    value = jnp.broadcast_to(value, (8, 256)).astype(BF)
    dbuf[tp] = dot(value, op[...]).astype(BF)
    to_tp(dbuf.at[tp], dbuf.at[tp], d_send, d_recv)

    swap_cache.wait_recv()
    expand(partner, 256)
    swap_rows.wait_recv()
    new_rows = nb[:, 0:512]
    keys = dot_t(ku[...], new_rows).astype(BF)
    vals = dot_t(vu[...], new_rows).astype(BF)
    unit = (
        lax.broadcasted_iota(jnp.int32, (32, 128), 0)
        == lax.broadcasted_iota(jnp.int32, (32, 128), 1)
    ).astype(F32).astype(BF)
    turned_keys = dot_t(unit, nb[:, 512:640]).astype(BF)
    for h in range(4):
        kbuf[h, 0:64, 512:640] = keys[64 * h : 64 * h + 64]
        kbuf[h, 64:96, 512:640] = turned_keys
        vbuf[h, 0:64, 512:640] = vals[64 * h : 64 * h + 64]

    slots = nz * ny
    count = slots * 4
    lane = lax.broadcasted_iota(jnp.int32, (1, 512), 1)
    key_place = jnp.where(lane < 256, kv * 256 + lane, other_kv * 256 + lane - 256)
    old = key_place < fill
    row = lax.broadcasted_iota(jnp.int32, (count, 128), 0)
    slot = lax.div(row, 4)
    src = lax.rem(lax.div(slot, ny) + z, nz) * ny + lax.rem(lax.rem(slot, ny) + y, ny)
    query_token = (src * 2 + core) * 4 + lax.rem(row, 4)
    lane = lax.broadcasted_iota(jnp.int32, (count, 128), 1)
    key_token = jnp.where(lane < 16, kv * 4 + lane, other_kv * 4 + lane - 16)
    fresh = (lax.rem(lane, 16) < 4) & (lane < 32) & (key_token <= query_token)

    many(qbuf.at[pl.ds(1, peers)], q_send, q_recv).wait_recv()
    mid[...] = qbuf[...].reshape(slots * 16, 128).astype(F32)
    for h in range(4):
        queries = mid[pl.ds(h, count, stride=4), :].astype(BF)
        s_old = jnp.where(old, dot(queries, kbuf[h, :, 0:512]), NEG)
        s_new = jnp.where(fresh, dot(queries, kbuf[h, :, 512:640]), NEG)
        peak = jnp.maximum(
            jnp.max(s_old, axis=-1, keepdims=True), jnp.max(s_new, axis=-1, keepdims=True)
        )
        w_old = jnp.exp2(s_old - peak).astype(BF)
        w_new = jnp.exp2(s_new - peak).astype(BF)
        out = dot_t(w_old, vbuf[h, :, 0:512]) + dot_t(w_new, vbuf[h, :, 512:640])
        first = peak.astype(BF).astype(F32)
        second = (peak - first).astype(BF).astype(F32)
        third = peak - first - second
        out = jnp.where(lane == 68, out - out.astype(BF).astype(F32), out)
        out = jnp.where(lane == 65, first, out)
        out = jnp.where(lane == 66, second, out)
        out = jnp.where(lane == 67, third, out)
        mid[pl.ds(h, count, stride=4), :] = out
    rsend[...] = mid[...].astype(BF).reshape(slots, 16, 128)
    rbuf[0] = rsend[0]

    for kv_t, place, slot in targets():
        pltpu.make_async_remote_copy(
            src_ref=rsend.at[place], dst_ref=rbuf.at[slot], send_sem=r_send, recv_sem=r_recv,
            device_id=(kv_t, tp), device_id_type=MESH,
        ).start()

    many(dbuf.at[pl.ds(0, ntp - 1)], d_send, d_recv).wait_recv()
    dec_sum = sum(dbuf[j].astype(F32) for j in range(ntp)).astype(BF)
    dec_out[...] = dec_sum[0:1]
    many(rbuf.at[pl.ds(1, peers)], r_send, r_recv).wait_recv()
    parts = rbuf[...].astype(F32)
    lane = lax.broadcasted_iota(jnp.int32, parts.shape, 2)
    peaks = jnp.sum(
        jnp.where((lane >= 65) & (lane < 68), parts, 0.0), axis=-1, keepdims=True
    )
    factor = jnp.exp2(peaks - jnp.max(peaks, axis=0, keepdims=True))
    merged = jnp.sum(parts * factor, axis=0)
    vs[...] = merged / (merged[:, 64:65] + merged[:, 68:69])
    value = jnp.concatenate([vs[pl.ds(h, 4, stride=4), :][:, 0:64] for h in range(4)], axis=1)
    obuf[tp] = dot(value.astype(BF), op[...]).astype(BF)
    to_tp(obuf.at[tp], obuf.at[tp], o_send, o_recv)
    many(obuf.at[pl.ds(0, ntp - 1)], o_send, o_recv).wait_recv()
    piece_out[...] = sum(obuf[j].astype(F32) for j in range(ntp)).astype(BF)

    many(cbuf.at[pl.ds(0, ntp - 1)], c_send, c_recv).wait_send()
    swap_cache.wait_send()
    swap_rows.wait_send()
    many(qbuf.at[pl.ds(1, peers)], q_send, q_recv).wait_send()
    many(dbuf.at[pl.ds(0, ntp - 1)], d_send, d_recv).wait_send()
    many(rbuf.at[pl.ds(1, peers)], r_send, r_recv).wait_send()
    many(obuf.at[pl.ds(0, ntp - 1)], o_send, o_recv).wait_send()


OUTS = ((4, 2048), (1, 2048), (4, 544), (1, 544))


def store(*refs):
    sems = refs[8]
    copies = [pltpu.make_async_copy(refs[i], refs[4 + i], sems.at[i]) for i in range(4)]
    for copy in copies:
        copy.start()
    for copy in copies:
        copy.wait()


def local(nz, ny, ntp, *args):
    (
        piece_tokens, decode_tokens, prompt_fill, decode_fill, prompt_cache, decode_cache,
        input_gain, query_gain, latent_gain, query_down, latent_down, rope_down,
        query_up, qrope_up, key_up, value_up, out_proj,
    ) = args
    slots = nz * ny
    operands = (
        prompt_fill[None], decode_fill[None], piece_tokens, decode_tokens,
        input_gain[None], query_gain, latent_gain[None],
        query_down.T, latent_down, rope_down.T, query_up, qrope_up,
        key_up.reshape(256, 512), value_up.transpose(0, 2, 1).reshape(256, 512),
        out_proj, prompt_cache.T, decode_cache[0].T,
    )
    copies = [pltpu.VMEM(a.shape, a.dtype) for a in operands]
    dma = pltpu.SemaphoreType.DMA
    any_spec = pl.BlockSpec(memory_space=pltpu.HBM)
    vmem_spec = pl.BlockSpec(memory_space=pltpu.VMEM)
    results = pl.pallas_call(
        functools.partial(kernel, nz, ny, ntp),
        out_shape=tuple(pltpu.VMEM(shape, BF) for shape in OUTS),
        in_specs=[any_spec] * len(operands),
        out_specs=[vmem_spec] * 4,
        scratch_shapes=copies
        + [
            pltpu.VMEM((544, 256), BF),
            pltpu.VMEM((8, 2048), F32),
            pltpu.VMEM((ntp, 8, 384), BF),
            pltpu.VMEM((128, 640), BF),
            pltpu.VMEM((32, 128), F32),
            pltpu.VMEM((4, 128, 640), BF),
            pltpu.VMEM((4, 128, 640), BF),
            pltpu.VMEM((slots, 16, 128), BF),
            pltpu.VMEM((slots, 16, 128), BF),
            pltpu.VMEM((slots, 16, 128), BF),
            pltpu.VMEM((slots * 16, 128), F32),
            pltpu.VMEM((16, 128), F32),
            pltpu.VMEM((ntp, 4, 2048), BF),
            pltpu.VMEM((ntp, 8, 2048), BF),
            pltpu.SemaphoreType.REGULAR,
            pltpu.SemaphoreType.REGULAR,
            pltpu.SemaphoreType.REGULAR,
            dma((len(operands),)),
        ]
        + [dma] * 14,
        compiler_params=pltpu.CompilerParams(collective_id=0, has_side_effects=True),
    )(*operands)
    return pl.pallas_call(
        store,
        out_shape=tuple(jax.ShapeDtypeStruct(shape, BF) for shape in OUTS),
        in_specs=[vmem_spec] * 4,
        out_specs=[any_spec] * 4,
        scratch_shapes=[dma((4,))],
    )(*(pltpu.with_memory_space_constraint(r, pltpu.VMEM) for r in results))


def solution(mesh):
    ntp = mesh.shape["tp"]
    chips = mesh.shape["kv"] // 2
    ny = 1
    while ny * ny < chips:
        ny *= 2
    placed = (
        P("kv", None), P("kv", None), P(), P("kv"), P("kv", None), P("kv", None, None),
        P(), P(), P(), P(None, "tp"), P(None, "tp"), P(), P(None, "tp"), P(None, "tp"),
        P("tp", None, None), P("tp", None, None), P("tp", None),
    )
    return jax.shard_map(
        functools.partial(local, chips // ny, ny, ntp),
        mesh=mesh,
        in_specs=placed,
        out_specs=(P("kv", None),) * 4,
        check_vma=False,
    )
```

time: 199 us -> 44.9 us (0.23)
  waiting for transfers between devices: 104 us -> 0 us
  Pallas kernels: 0 us -> 42.6 us
  blocking collectives: 22.7 us -> 0 us
  matrix products: 17.1 us -> 0 us
  local copies, waits for them, and re-layouts: 15.1 us -> 0 us
  between operations: 16.5 us -> 1.94 us
  other arithmetic: 12.4 us -> 0 us
  starting transfers between devices: 9.7 us -> 0 us
    all_gather x1 -> x0, waiting for transfers between devices: 79.9 us -> none  [gather_packed(): lines, at, finished = (lax.all_gather(flat, axis), 0, [])]
    pallas_call x0 -> x2, Pallas kernels: none -> 42.6 us  [the longest x1 41.9 us: local(): pl.pallas_call(functools.partial(kernel, nz, ny, ntp), out_shape=tuple((p...]
    all_to_all x1 -> x0, waiting for transfers between devices: 24.6 us -> none  [sent_together(): lax.all_to_all(both, axis, split_axis=split_dim, concat_axis=concat_dim,...]
    dot_general x17 -> x0, matrix products: 17.1 us -> none  [the longest x2 3.46 us: block_attend(): jnp.einsum('nhl,sl->nhs', absorbed, latent_keys, preferred_element_type=j...]
    unnamed x1 -> x0, blocking collectives: 13.9 us -> none
    all_to_all x1 -> x0, starting transfers between devices: 9.66 us -> none  [sent_together(): lax.all_to_all(both, axis, split_axis=split_dim, concat_axis=concat_dim,...]
    all_to_all x1 -> x0, blocking collectives: 8.8 us -> none  [from_everyone(): return lax.all_to_all(copies, axis, split_axis=0, concat_axis=0, tiled=True)]
    unnamed x44 -> x0, local copies, waits for them, and re-layouts: 7.06 us -> none
  transfers between devices with their start and end apart: 2 -> 0, of which waited for: 2 -> 0; matrix products, arithmetic and copies ran while one was open for 6% -> 0% of each run, Pallas kernels for 0% -> 0%
where the time goes in v1:
time: 44.9 us; the launch traced here: 44.5 us
  Pallas kernels  42.6 us (95%)
  between operations  1.94 us (4%)
    pallas_call x1, Pallas kernels, local(): pl.pallas_call(functools.partial(kernel, nz, ny, ntp), out_shape=tuple((p...  41.9 us

profile of v1, /device:TPU:1, one launch (start us, length us, event | category | flops | bytes accessed | tf_op | source)
XLA Modules:
  0.0 44.5 jit_solution(5495504324247720074)
XLA Ops:
  1.9 41.9 %shard_map.192 = (bf16[4,2048]{1,0:T(4,128)(2,1)S(1)}, bf16[1,2048]{1,0:T(2,128)(2,1)S(1)}, bf16[4,544]{1,0:T(4,128)(2,1)S(1)}, bf16[1,544]{1,0:T(2,128)(2,1)S(1)}) custom-call(s32[1,1]{1,0:T(1,128)} %bitcast.14.fill_any, s32[1,1]{1,0:T(1,128)} %bitcast.15.dfill_any, bf16[4,2048]{1,0:T(4,128)(2,1)} %piece_any.1, bf16[1,2048]{1,0:T(2,128)(2,1)} %dec_any.1, ...), custom_call_target="tpu_custom_call" | custom-call | tf_op jit(solution)/shard_map/pallas_call | solution.py:376
  43.9 0.6 %shard_map.193 = (bf16[4,2048]{1,0:T(4,128)(2,1)}, bf16[1,2048]{1,0:T(2,128)(2,1)}, bf16[4,544]{1,0:T(4,128)(2,1)}, bf16[1,544]{1,0:T(2,128)(2,1)}) custom-call(bf16[4,2048]{1,0:T(4,128)(2,1)S(1)} %get-tuple-element.8.refs_0_, bf16[1,2048]{1,0:T(2,128)(2,1)S(1)} %get-tuple-element.9.refs_1_, bf16[4,544]{1,0:T(4,128)(2,1)S(1)} %get-tuple-element.10.refs_2_, ...), custom_call_target="tpu_custom_call" | custom-call | tf_op jit(solution)/shard_map/pallas_call | solution.py:405

commit v2 on v1

v2 whole, which is shorter than its diff:
```python
import functools

import jax
import jax.numpy as jnp
from jax import lax
from jax.experimental import pallas as pl
from jax.experimental.pallas import tpu as pltpu
from jax.sharding import PartitionSpec as P

MESH = pl.DeviceIdType.MESH
NEG = -1e30
BLOCKS = 2
CHUNK = 32
EPS = 1e-06
LOG2E = 1.4426950408889634
SCALE = (64 + 32) ** (-0.5) * LOG2E
INVERSE = tuple(float(10000.0 ** (-i / 16)) for i in range(16))
BF = jnp.bfloat16
F32 = jnp.float32


def dot(a, b):
    return jnp.dot(a, b, preferred_element_type=F32)


def dot_t(a, b):
    return lax.dot_general(a, b, (((1,), (1,)), ((), ())), preferred_element_type=F32)


def angles(places):
    lane = lax.broadcasted_iota(jnp.int32, (8, 128), 1)
    step = lax.rem(lane, 16)
    inverse = jnp.full((8, 128), INVERSE[0], F32)
    for i in range(1, 16):
        inverse = jnp.where(step == i, INVERSE[i], inverse)
    turn = places.astype(F32) * inverse
    sine = jnp.sin(turn)
    return jnp.cos(turn), jnp.where(lax.rem(lane, 32) < 16, -sine, sine)


def rotate(values, cosine, sine):
    lane = lax.broadcasted_iota(jnp.int32, (8, 128), 1)
    other = jnp.where(
        lax.rem(lane, 32) < 16, pltpu.roll(values, 112, 1), pltpu.roll(values, 16, 1)
    )
    return values * cosine + other * sine


def kernel(
    nz, ny, ntp,
    fill_any, dfill_any, piece_any, dec_any, ingain_any, qgain_any, lgain_any,
    qd_any, ld_any, rd_any, qu_any, qr_any, ku_any, vu_any, op_any, pc_any, dc_any,
    piece_out, dec_out, piece_rows, dec_rows,
    fill_v, dfill_v, piece_v, dec_v, ingain_v, qgain_v, lgain_v,
    qd, ld, rd, qu, qr, ku, vu, op, pc, dc,
    partner, xs, cbuf, nb, kbuf, vbuf, qbuf, rsend, rbuf, psend, pbuf, mid, scores, weights, terms, vs, obuf, dbuf,
    chip_in, line_in, all_in,
    load_sem, c_send, c_recv, p_send, p_recv, n_send, n_recv,
    q_send, q_recv, r_send, r_recv, s_send, s_recv, o_send, o_recv, d_send, d_recv,
):
    kv, tp = lax.axis_index("kv"), lax.axis_index("tp")
    chip, core = lax.div(kv, 2), lax.rem(kv, 2)
    z, y = lax.div(chip, ny), lax.rem(chip, ny)
    peers = nz * ny - 1
    other_kv = chip * 2 + (1 - core)

    pairs = (
        (piece_any, piece_v), (dec_any, dec_v), (ingain_any, ingain_v), (qd_any, qd),
        (ld_any, ld), (pc_any, pc), (ku_any, ku), (vu_any, vu), (rd_any, rd),
        (fill_any, fill_v), (dfill_any, dfill_v), (qgain_any, qgain_v), (lgain_any, lgain_v),
        (qu_any, qu), (qr_any, qr), (dc_any, dc), (op_any, op),
    )
    loads = [pltpu.make_async_copy(a, v, load_sem.at[i]) for i, (a, v) in enumerate(pairs)]
    barrier = pltpu.get_barrier_semaphore()

    z_order = [(p + 1) // 2 if p % 2 else -(p // 2) % nz for p in range(nz)]

    def slot_of(dz, dy):
        return z_order.index(dz % nz) * ny + dy % ny

    z_part = [lax.rem(z + d, nz) * (2 * ny) + core for d in range(nz)]
    y_part = [lax.rem(y + d, ny) * 2 for d in range(ny)]

    def targets():
        def far(step):
            dz, dy = step
            return -(min(dz, nz - dz) + min(dy, ny - dy))

        steps = [(dz, dy) for dz in range(nz) for dy in range(ny)][1:]
        for dz, dy in sorted(steps, key=far):
            yield z_part[dz] + y_part[dy], slot_of(dz, dy), slot_of(-dz, -dy)

    def tell(sem, kv_t, tp_t):
        pl.semaphore_signal(sem, inc=1, device_id=(kv_t, tp_t), device_id_type=MESH)

    beside = sorted(range(1, ntp), key=lambda j: -min(j, ntp - j))

    @pl.when(core == 0)
    def _():
        for j in beside:
            tell(barrier, kv, lax.rem(tp + j, ntp))

    @pl.when(core == 1)
    def _():
        tell(barrier, other_kv, tp)

    for load in loads[:5]:
        load.start()


    @pl.when(core == 0)
    def _():
        pl.semaphore_wait(barrier, ntp)
        tell(chip_in, other_kv, tp)
        for j in beside:
            tell(line_in, kv, lax.rem(tp + j, ntp))

    @pl.when(core == 1)
    def _():
        pl.semaphore_wait(chip_in, 1)
        for kv_t, unused, unused_too in targets():
            tell(barrier, kv_t, tp)

    for load in loads[5:]:
        load.start()

    kbuf[...] = jnp.zeros(kbuf.shape, BF)
    nb[0:16] = jnp.zeros((16, 640), BF)
    nb[32:128] = jnp.zeros((96, 640), BF)
    xs[...] = jnp.zeros(xs.shape, F32)
    for load in loads[:5]:
        load.wait()
    xs[0:4] = piece_v[...].astype(F32)
    xs[4:5] = dec_v[...].astype(F32)
    x = xs[...]
    mean = jnp.mean(x * x, axis=-1, keepdims=True)
    normed = (x * lax.rsqrt(mean + EPS) * ingain_v[...]).astype(BF)
    cbuf[tp, :, 0:128] = dot(normed, ld[...]).astype(BF)
    cbuf[tp, :, 128:320] = dot_t(normed, qd[...]).astype(BF)

    @pl.when(core == 0)
    def _():
        pl.semaphore_wait(line_in, ntp - 1)
        tell(chip_in, other_kv, tp)

    @pl.when(core == 1)
    def _():
        pl.semaphore_wait(chip_in, 1)

    def to_tp(src, dst, send, recv):
        for j in beside:
            pltpu.make_async_remote_copy(
                src_ref=src, dst_ref=dst, send_sem=send, recv_sem=recv,
                device_id=(kv, lax.rem(tp + j, ntp)), device_id_type=MESH,
            ).start()

    def to_partner(src, dst, send, recv):
        return pltpu.make_async_remote_copy(
            src_ref=src, dst_ref=dst, send_sem=send, recv_sem=recv,
            device_id=(other_kv, tp), device_id_type=MESH,
        )

    def many(ref, send, recv):
        return to_partner(ref, ref, send, recv)

    to_tp(cbuf.at[tp], cbuf.at[tp], c_send, c_recv)
    loads[5].wait()
    swap_cache = to_partner(pc, partner, p_send, p_recv)
    swap_cache.start()

    for load in loads[6:9]:
        load.wait()

    def keep_keys(keys, turned_keys, at):
        width = keys.shape[1]
        for h in range(4):
            own, rope = h % 2 * 64, 128 + 32 * h
            kbuf[h, own : own + 64, at : at + width] = keys[64 * h : 64 * h + 64]
            kbuf[h, rope : rope + 32, at : at + width] = turned_keys

    def keep_values(vals, at):
        half = lax.div(lax.broadcasted_iota(jnp.int32, (vals.shape[0], 128), 1), 64)
        for h in range(4):
            pair = vals[:, h // 2 * 128 : h // 2 * 128 + 128]
            vbuf[h, at : at + vals.shape[0]] = jnp.where(half == h % 2, pair, 0.0).astype(BF)

    def expand(rows, at):
        latent = rows[0:512]
        keys = dot(ku[...], latent).astype(BF)
        turned_keys = rows[512:544]
        keep_keys(keys, turned_keys, at)
        keep_values(dot(vu[...], latent).T, at)

    expand(pc, 0)
    rope_raw = dot_t(normed, rd[...]).astype(BF).astype(F32)
    for load in loads[9:]:
        load.wait()
    fill, dfill = fill_v[...], dfill_v[...]
    token_row = lax.broadcasted_iota(jnp.int32, (8, 128), 0)
    places = jnp.where(token_row < 4, fill + kv * 4 + token_row, dfill)
    cosine, sine = angles(places)
    rope_row = rotate(
        jnp.concatenate([rope_raw, jnp.zeros((8, 96), F32)], axis=1), cosine, sine
    ).astype(BF)

    many(cbuf.at[pl.ds(0, ntp - 1)], c_send, c_recv).wait_recv()

    parts = [cbuf[j] for j in range(ntp)]
    lat = [p[:, 0:128].astype(F32) for p in parts]
    com = [p[:, 128:320].astype(F32) for p in parts]
    lat_mean = sum(jnp.sum(v * v, axis=-1, keepdims=True) for v in lat) / (128.0 * ntp)
    com_mean = sum(jnp.sum(v * v, axis=-1, keepdims=True) for v in com) / (192.0 * ntp)
    lat_scale, com_scale = lax.rsqrt(lat_mean + EPS), lax.rsqrt(com_mean + EPS)
    nope = jnp.zeros((8, 256), F32)
    turned = jnp.zeros((8, 128), F32)
    for j in range(ntp):
        part = (com[j] * com_scale * qgain_v[192 * j : 192 * j + 192][None]).astype(BF)
        nope += dot(part, qu[192 * j : 192 * j + 192])
        turned += dot(part, qr[192 * j : 192 * j + 192])
    turned = rotate(turned.astype(BF).astype(F32), cosine, sine) * SCALE
    nope = nope * SCALE
    qbuf[0, 0] = nope[0:4, 0:128].astype(BF)
    qbuf[0, 1] = nope[0:4, 128:256].astype(BF)
    qbuf[0, 2] = turned[0:4].astype(BF)

    @pl.when(core == 0)
    def _():
        pl.semaphore_wait(all_in, 1)

    @pl.when(core == 1)
    def _():
        pl.semaphore_wait(barrier, peers)
        tell(all_in, other_kv, tp)

    for kv_t, unused, slot in targets():
        pltpu.make_async_remote_copy(
            src_ref=qbuf.at[0], dst_ref=qbuf.at[slot],
            send_sem=q_send, recv_sem=q_recv.at[slot // (nz * ny // BLOCKS)],
            device_id=(kv_t, tp), device_id_type=MESH,
        ).start()

    for j in range(ntp):
        rows = (lat[j] * lat_scale * lgain_v[:, 128 * j : 128 * j + 128]).astype(BF)
        nb[0:8, 128 * j : 128 * j + 128] = rows
        piece_rows[:, 128 * j : 128 * j + 128] = rows[0:4]
        dec_rows[:, 128 * j : 128 * j + 128] = rows[4:5]
    nb[0:8, 512:640] = rope_row
    piece_rows[:, 512:544] = rope_row[0:4, 0:32]
    dec_rows[:, 512:544] = rope_row[4:5, 0:32]
    swap_rows = to_partner(nb.at[pl.ds(0, 16)], nb.at[pl.ds(16, 16)], n_send, n_recv)
    swap_rows.start()

    head = lax.broadcasted_iota(jnp.int32, (8, 256), 0)
    mine = lax.div(lax.broadcasted_iota(jnp.int32, (8, 256), 1), 64) == head
    alone = jnp.where(mine, jnp.broadcast_to(nope[4:5], (8, 256)), 0.0).astype(BF)
    absorbed = dot(alone, ku[...]).astype(BF)
    dec_turned = jnp.where(
        lax.div(lax.broadcasted_iota(jnp.int32, (8, 128), 1), 32) == token_row, turned[4:5], 0.0
    )
    dec_turned = dec_turned + pltpu.roll(dec_turned, 64, 1)
    dec_turned = (dec_turned + pltpu.roll(dec_turned, 96, 1))[:, 0:32].astype(BF)
    dec_scores = dot(absorbed, dc[0:512]) + dot(dec_turned, dc[512:544])
    spot = lax.broadcasted_iota(jnp.int32, dec_scores.shape, 1)
    dec_scores = jnp.where(spot < dfill, dec_scores, NEG)
    new_lat = nb[0:8, 0:512].astype(F32)[4:5]
    new_rope = rope_row.astype(F32)[4:5, 0:32]
    new_score = jnp.sum(absorbed.astype(F32) * new_lat, axis=-1, keepdims=True) + jnp.sum(
        dec_turned.astype(F32) * new_rope, axis=-1, keepdims=True
    )
    peak = jnp.maximum(jnp.max(dec_scores, axis=-1, keepdims=True), new_score)
    dec_weights = jnp.exp2(dec_scores - peak)
    new_weight = jnp.exp2(new_score - peak)
    total = jnp.sum(dec_weights, axis=-1, keepdims=True) + new_weight
    mixed = dot_t(dec_weights.astype(BF), dc[0:512]) + new_weight * new_lat
    value = dot_t(mixed.astype(BF), vu[...]) / total
    value = jnp.sum(jnp.where(mine, value, 0.0), axis=0, keepdims=True)
    value = jnp.broadcast_to(value, (8, 256)).astype(BF)
    dbuf[tp] = dot(value, op[...]).astype(BF)
    to_tp(dbuf.at[tp], dbuf.at[tp], d_send, d_recv)

    swap_cache.wait_recv()
    expand(partner, 256)
    swap_rows.wait_recv()
    new_rows = nb[:, 0:512]
    keys = dot_t(ku[...], new_rows).astype(BF)
    keep_values(dot_t(new_rows, vu[...]), 512)
    unit = (
        lax.broadcasted_iota(jnp.int32, (32, 128), 0)
        == lax.broadcasted_iota(jnp.int32, (32, 128), 1)
    ).astype(F32).astype(BF)
    turned_keys = dot_t(unit, nb[:, 512:640]).astype(BF)
    keep_keys(keys, turned_keys, 512)

    lane = lax.broadcasted_iota(jnp.int32, (1, 512), 1)
    key_place = jnp.where(lane < 256, kv * 256 + lane, other_kv * 256 + lane - 256)
    old = key_place < fill
    slots = nz * ny // BLOCKS
    count = slots * 4
    row = lax.broadcasted_iota(jnp.int32, (count, 128), 0)
    lane = lax.broadcasted_iota(jnp.int32, (count, 128), 1)
    key_token = jnp.where(lane < 16, kv * 4 + lane, other_kv * 4 + lane - 16)
    within = jnp.where(lane < 32, lax.rem(lane, 16) - 4 * lax.rem(row, 4), -1)
    is_new = (lax.rem(lane, 16) < 4) & (lane < 32)

    def attend(block):
        base = block * slots
        slot = lax.div(row, 4) + base
        turn = lax.div(slot, ny)
        dz = jnp.where(
            lax.rem(turn, 2) == 1, lax.div(turn + 1, 2), lax.rem(nz - lax.div(turn, 2), nz)
        )
        src = lax.rem(dz + z, nz) * ny + lax.rem(lax.rem(slot, ny) + y, ny)
        query_token = (src * 2 + core) * 4 + lax.rem(row, 4)
        fresh = is_new & (key_token <= query_token)
        got = [
            qbuf[base : base + slots, g].astype(F32).reshape(count, 128).astype(BF) for g in range(3)
        ]
        for h in range(4):
            queries = jnp.concatenate([got[h // 2], got[2]], axis=1)
            scores[h] = dot(queries, kbuf[h])
        for at in range(0, count, CHUNK):
            part = slice(at, at + CHUNK)
            scalars = jnp.zeros((CHUNK, 128), F32)
            for h in range(4):
                s_old = jnp.where(old, scores[h, part, 0:512], NEG)
                s_new = jnp.where(fresh[part], scores[h, part, 512:640], NEG)
                peak = jnp.ceil(
                    jnp.maximum(
                        jnp.max(s_old, axis=-1, keepdims=True),
                        jnp.max(s_new, axis=-1, keepdims=True),
                    )
                )
                w_old = jnp.exp2(s_old - peak)
                w_new = jnp.exp2(s_new - peak)
                total = jnp.sum(w_old, axis=-1, keepdims=True) + jnp.sum(
                    w_new, axis=-1, keepdims=True
                )
                weights[h, part, 0:512] = w_old.astype(BF)
                weights[h, part, 512:640] = w_new.astype(BF)
                scalar = jnp.where(lane[part] < 16, peak, total)
                scalars = jnp.where(within[part] == h, scalar, scalars)
            terms[part] = scalars
        for pair in range(2):
            h = 2 * pair
            mid[pl.ds(pair, count, stride=2), :] = dot(weights[h], vbuf[h]) + dot(
                weights[h + 1], vbuf[h + 1]
            )
        rsend[base : base + slots] = mid[...].astype(BF).reshape(slots, 8, 128)
        gather = lax.div(lax.broadcasted_iota(jnp.int32, (slots, count), 1), 4)
        gather = gather == lax.broadcasted_iota(jnp.int32, (slots, count), 0)
        rows = jnp.dot(
            gather.astype(F32), terms[...],
            preferred_element_type=F32, precision=lax.Precision.HIGHEST,
        )
        psend[base : base + slots] = rows[:, None, :]

    for block in reversed(range(BLOCKS)):
        base = block * slots
        first = max(base, 1)
        many(qbuf.at[pl.ds(first, base + slots - first)], q_send, q_recv.at[block]).wait_recv()
        attend(block)
        if block == 0:
            rbuf[0] = rsend[0]
            pbuf[0] = psend[0]
        for kv_t, place, slot in targets():
            if place // slots == block:
                pltpu.make_async_remote_copy(
                    src_ref=rsend.at[place], dst_ref=rbuf.at[slot],
                    send_sem=r_send, recv_sem=r_recv,
                    device_id=(kv_t, tp), device_id_type=MESH,
                ).start()
                pltpu.make_async_remote_copy(
                    src_ref=psend.at[place], dst_ref=pbuf.at[slot],
                    send_sem=s_send, recv_sem=s_recv,
                    device_id=(kv_t, tp), device_id_type=MESH,
                ).start()

    many(dbuf.at[pl.ds(0, ntp - 1)], d_send, d_recv).wait_recv()
    dec_sum = sum(dbuf[j].astype(F32) for j in range(ntp)).astype(BF)
    dec_out[...] = dec_sum[0:1]
    many(rbuf.at[pl.ds(1, peers)], r_send, r_recv).wait_recv()
    many(pbuf.at[pl.ds(1, peers)], s_send, s_recv).wait_recv()
    scalars = pbuf[...]
    factor = jnp.exp2(scalars - jnp.max(scalars, axis=0, keepdims=True))
    totals = pltpu.roll(scalars, 112, 2)
    every = scalars.shape[0]
    lane = lax.broadcasted_iota(jnp.int32, (1, 1, 128), 2)
    factor = jnp.where(lane < 16, factor, 0.0)
    total = jnp.sum(factor * totals, axis=0)
    mine = lax.div(lax.broadcasted_iota(jnp.int32, (1, 8, 128), 2), 2)
    mine = mine == lax.broadcasted_iota(jnp.int32, (1, 8, 128), 1)
    spread = lax.rem(lax.broadcasted_iota(jnp.int32, (128, 128), 0), 2)
    spread = spread == lax.div(lax.broadcasted_iota(jnp.int32, (128, 128), 1), 64)
    spread = spread.astype(F32)
    factor = jnp.where(mine, factor, 0.0).reshape(every * 8, 128).astype(BF)
    factor = dot(factor, spread.astype(BF)).reshape(every, 8, 128)
    total = jnp.dot(
        jnp.where(mine[0], total, 0.0), spread,
        preferred_element_type=F32, precision=lax.Precision.HIGHEST,
    )
    merged = jnp.sum(rbuf[...].astype(F32) * factor, axis=0)
    vs[...] = merged / total
    value = jnp.concatenate([vs[pl.ds(p, 4, stride=2), :] for p in range(2)], axis=1)
    obuf[tp] = dot(value.astype(BF), op[...]).astype(BF)
    to_tp(obuf.at[tp], obuf.at[tp], o_send, o_recv)
    many(obuf.at[pl.ds(0, ntp - 1)], o_send, o_recv).wait_recv()
    piece_out[...] = sum(obuf[j].astype(F32) for j in range(ntp)).astype(BF)

    many(cbuf.at[pl.ds(0, ntp - 1)], c_send, c_recv).wait_send()
    swap_cache.wait_send()
    swap_rows.wait_send()
    many(qbuf.at[pl.ds(1, peers)], q_send, q_recv.at[0]).wait_send()
    many(dbuf.at[pl.ds(0, ntp - 1)], d_send, d_recv).wait_send()
    many(rbuf.at[pl.ds(1, peers)], r_send, r_recv).wait_send()
    many(pbuf.at[pl.ds(1, peers)], s_send, s_recv).wait_send()
    many(obuf.at[pl.ds(0, ntp - 1)], o_send, o_recv).wait_send()


OUTS = ((4, 2048), (1, 2048), (4, 544), (1, 544))


def store(*refs):
    sems = refs[8]
    copies = [pltpu.make_async_copy(refs[i], refs[4 + i], sems.at[i]) for i in range(4)]
    for copy in copies:
        copy.start()
    for copy in copies:
        copy.wait()


def local(nz, ny, ntp, *args):
    (
        piece_tokens, decode_tokens, prompt_fill, decode_fill, prompt_cache, decode_cache,
        input_gain, query_gain, latent_gain, query_down, latent_down, rope_down,
        query_up, qrope_up, key_up, value_up, out_proj,
    ) = args
    slots = nz * ny
    operands = (
        prompt_fill[None], decode_fill[None], piece_tokens, decode_tokens,
        input_gain[None], query_gain, latent_gain[None],
        query_down.T, latent_down, rope_down.T, query_up, qrope_up,
        key_up.reshape(256, 512), value_up.transpose(0, 2, 1).reshape(256, 512),
        out_proj, prompt_cache.T, decode_cache[0].T,
    )
    copies = [pltpu.VMEM(a.shape, a.dtype) for a in operands]
    dma = pltpu.SemaphoreType.DMA
    any_spec = pl.BlockSpec(memory_space=pltpu.HBM)
    vmem_spec = pl.BlockSpec(memory_space=pltpu.VMEM)
    results = pl.pallas_call(
        functools.partial(kernel, nz, ny, ntp),
        out_shape=tuple(pltpu.VMEM(shape, BF) for shape in OUTS),
        in_specs=[any_spec] * len(operands),
        out_specs=[vmem_spec] * 4,
        scratch_shapes=copies
        + [
            pltpu.VMEM((544, 256), BF),
            pltpu.VMEM((8, 2048), F32),
            pltpu.VMEM((ntp, 8, 384), BF),
            pltpu.VMEM((128, 640), BF),
            pltpu.VMEM((4, 256, 640), BF),
            pltpu.VMEM((4, 640, 128), BF),
            pltpu.VMEM((slots, 3, 4, 128), BF),
            pltpu.VMEM((slots, 8, 128), BF),
            pltpu.VMEM((slots, 8, 128), BF),
            pltpu.VMEM((slots, 1, 128), F32),
            pltpu.VMEM((slots, 1, 128), F32),
            pltpu.VMEM((slots // BLOCKS * 8, 128), F32),
            pltpu.VMEM((4, slots // BLOCKS * 4, 640), F32),
            pltpu.VMEM((4, slots // BLOCKS * 4, 640), BF),
            pltpu.VMEM((slots // BLOCKS * 4, 128), F32),
            pltpu.VMEM((8, 128), F32),
            pltpu.VMEM((ntp, 4, 2048), BF),
            pltpu.VMEM((ntp, 8, 2048), BF),
            pltpu.SemaphoreType.REGULAR,
            pltpu.SemaphoreType.REGULAR,
            pltpu.SemaphoreType.REGULAR,
            dma((len(operands),)),
        ]
        + [dma] * 7
        + [dma((BLOCKS,))]
        + [dma] * 8,
        compiler_params=pltpu.CompilerParams(collective_id=0, has_side_effects=True),
    )(*operands)
    return pl.pallas_call(
        store,
        out_shape=tuple(jax.ShapeDtypeStruct(shape, BF) for shape in OUTS),
        in_specs=[vmem_spec] * 4,
        out_specs=[any_spec] * 4,
        scratch_shapes=[dma((4,))],
    )(*(pltpu.with_memory_space_constraint(r, pltpu.VMEM) for r in results))


def solution(mesh):
    ntp = mesh.shape["tp"]
    chips = mesh.shape["kv"] // 2
    ny = 1
    while ny * ny < chips:
        ny *= 2
    placed = (
        P("kv", None), P("kv", None), P(), P("kv"), P("kv", None), P("kv", None, None),
        P(), P(), P(), P(None, "tp"), P(None, "tp"), P(), P(None, "tp"), P(None, "tp"),
        P("tp", None, None), P("tp", None, None), P("tp", None),
    )
    return jax.shard_map(
        functools.partial(local, chips // ny, ny, ntp),
        mesh=mesh,
        in_specs=placed,
        out_specs=(P("kv", None),) * 4,
        check_vma=False,
    )
```

time: 44.9 us -> 41.3 us (0.920)
  the two profiles are of different devices: /device:TPU:1 before, /device:TPU:8 now
where the time goes in v2:
time: 41.3 us; the launch traced here: 41.1 us
  Pallas kernels  39.2 us (95%)
  between operations  1.94 us (5%)
    pallas_call x1, Pallas kernels, local(): pl.pallas_call(functools.partial(kernel, nz, ny, ntp), out_shape=tuple((p...  38.5 us

profile of v2, /device:TPU:8, one launch (start us, length us, event | category | flops | bytes accessed | tf_op | source)
XLA Modules:
  0.0 41.1 jit_solution(6999093936155129310)
XLA Ops:
  1.9 38.5 %shard_map.192 = (bf16[4,2048]{1,0:T(4,128)(2,1)S(1)}, bf16[1,2048]{1,0:T(2,128)(2,1)S(1)}, bf16[4,544]{1,0:T(4,128)(2,1)S(1)}, bf16[1,544]{1,0:T(2,128)(2,1)S(1)}) custom-call(s32[1,1]{1,0:T(1,128)} %bitcast.14.fill_any, s32[1,1]{1,0:T(1,128)} %bitcast.15.dfill_any, bf16[4,2048]{1,0:T(4,128)(2,1)} %piece_any.1, bf16[1,2048]{1,0:T(2,128)(2,1)} %dec_any.1, ...), custom_call_target="tpu_custom_call" | custom-call | tf_op jit(solution)/shard_map/pallas_call | solution.py:449
  40.5 0.6 %shard_map.193 = (bf16[4,2048]{1,0:T(4,128)(2,1)}, bf16[1,2048]{1,0:T(2,128)(2,1)}, bf16[4,544]{1,0:T(4,128)(2,1)}, bf16[1,544]{1,0:T(2,128)(2,1)}) custom-call(bf16[4,2048]{1,0:T(4,128)(2,1)S(1)} %get-tuple-element.8.refs_0_, bf16[1,2048]{1,0:T(2,128)(2,1)S(1)} %get-tuple-element.9.refs_1_, bf16[4,544]{1,0:T(4,128)(2,1)S(1)} %get-tuple-element.10.refs_2_, ...), custom_call_target="tpu_custom_call" | custom-call | tf_op jit(solution)/shard_map/pallas_call | solution.py:484
